TPU v7x, 32 devices: a whole 2x2x4 slice. The times are simulated.
32 devices in a mesh: dp: 2 (over y), kv: 16 (over z, x, core), tp: 1.
Axes of the slice: x: 2, y: 2, z: 4, core: 2. Of those that a mesh axis runs over, the one named last changes fastest.
Arguments:
- tokens: bfloat16 [16, 4096], P('dp', 'kv'), may hold values from -6 to 6
- attn_gain: float32 [4096], P('kv'), may hold values from 0.1 to 1.9
- query_weight: bfloat16 [4096, 2048], P('kv', 'tp'), may hold values from -0.09375 to 0.09375
- key_cache: bfloat16 [16, 2048, 8, 2, 128], P('dp', 'kv', 'tp'), may hold values from -1024 to 1024
- value_cache: bfloat16 [16, 2048, 8, 256], P('dp', 'kv', 'tp'), may hold values from -6 to 6
- lambdas: float32 [8], P('tp'), may hold values from 0.3 to 0.8
- head_gain: float32 [256], replicated, may hold values from 0.1 to 1.9
- out_weight: bfloat16 [2048, 4096], P('tp', 'kv'), may hold values from -0.125 to 0.125
- mixer_gain: float32 [4096], P('kv'), may hold values from 0.1 to 1.9
- up_weight: bfloat16 [4096, 16384], P('kv', 'tp'), may hold values from -0.09375 to 0.09375
- down_weight: bfloat16 [16384, 4096], P('tp', 'kv'), may hold values from -0.046875 to 0.046875
Outputs:
- result: bfloat16 [16, 4096], P('dp', 'kv')
All inputs are finite; a program needn't handle non-finite values.
Results may differ from a plain program's by a relative error of at most 0.024.
Values may be sent and summed in bfloat16 or wider, within the bound.
A program may use at most 64 MiB of HBM per device.

v0:
```python
import math
import jax
import jax.numpy as jnp
from jax import lax
from jax.sharding import PartitionSpec as P

D = 4096
EPS = 1e-05


def merged(value, axis, combine):
    everything = jax.tree.map(lambda part: lax.all_gather(part, axis), value)
    initial = jax.tree.map(lambda part: part[0], everything)

    def lap(k, so_far):
        return combine(so_far, jax.tree.map(lambda part: part[k], everything))

    return lax.fori_loop(1, lax.axis_size(axis), lap, initial)


def rotate(query, position):
    half = query.shape[-1] // 2
    inverse = 10000.0 ** (-jnp.arange(half, dtype=jnp.float32) / half)
    angle = jnp.float32(position) * inverse
    cosine = jnp.cos(angle)
    sine = jnp.sin(angle)
    first = query[..., :half]
    second = query[..., half:]
    return jnp.concatenate(
        [first * cosine - second * sine, second * cosine + first * sine], axis=-1
    )


def combine_partial(earlier, later):
    top_a, total_a, numer_a = earlier
    top_b, total_b, numer_b = later
    top = jnp.maximum(top_a, top_b)
    factor_a = jnp.exp(top_a - top)
    factor_b = jnp.exp(top_b - top)
    return (
        top,
        total_a * factor_a + total_b * factor_b,
        numer_a * factor_a[..., None] + numer_b * factor_b[..., None],
    )


def local(
    tokens,
    attn_gain,
    query_weight,
    key_cache,
    value_cache,
    lambdas,
    head_gain,
    out_weight,
    mixer_gain,
    up_weight,
    down_weight,
):
    row_count = tokens.shape[0]
    local_heads = key_cache.shape[2]
    head_width = key_cache.shape[4]
    length = key_cache.shape[1] * lax.axis_size("kv")
    tok_float = tokens.astype(jnp.float32)
    own_squares = jnp.sum(tok_float * tok_float, axis=1)
    scaled_in = (tok_float * attn_gain).astype(jnp.bfloat16)
    query_part = jnp.dot(scaled_in, query_weight, preferred_element_type=jnp.float32)
    squares = lax.psum(own_squares, "kv")
    query_raw = lax.psum(query_part, "kv")
    attn_inv = lax.rsqrt(squares / D + EPS)
    shaped = (attn_inv[:, None] * query_raw).reshape(row_count, local_heads, 2, head_width)
    query = rotate(shaped, length - 1).astype(jnp.bfloat16)
    scores = jnp.einsum(
        "bhcd,bkhcd->bhck", query, key_cache, preferred_element_type=jnp.float32
    ) / math.sqrt(head_width)
    top = jnp.max(scores, axis=-1)
    expo = jnp.exp(scores - top[..., None])
    denom = jnp.sum(expo, axis=-1)
    numer = jnp.einsum(
        "bhck,bkhv->bhcv",
        expo.astype(jnp.bfloat16),
        value_cache,
        preferred_element_type=jnp.float32,
    )
    top, denom, numer = merged((top, denom, numer), "kv", combine_partial)
    ratio = numer / denom[..., None]
    mixed = ratio[:, :, 0] - lambdas[None, :, None] * ratio[:, :, 1]
    normed = mixed * lax.rsqrt(jnp.mean(mixed * mixed, axis=-1, keepdims=True) + EPS) * head_gain
    normed = normed.astype(jnp.bfloat16).reshape(row_count, -1)
    attn_part = jnp.dot(normed, out_weight, preferred_element_type=jnp.float32)
    attn_out = lax.psum(attn_part, "tp")
    middle = (tok_float + attn_out).astype(jnp.bfloat16)
    mid_float = middle.astype(jnp.float32)
    mix_squares = lax.psum(jnp.sum(mid_float * mid_float, axis=1), "kv")
    mixer_inv = lax.rsqrt(mix_squares / D + EPS)
    mixer_in = (mid_float * mixer_gain).astype(jnp.bfloat16)
    up_part = jnp.dot(mixer_in, up_weight, preferred_element_type=jnp.float32)
    share = lax.psum_scatter(up_part, "kv", scatter_dimension=1, tiled=True)
    hidden_share = jnp.square(jax.nn.relu(mixer_inv[:, None] * share)).astype(jnp.bfloat16)
    mixer_part = jnp.dot(
        lax.all_gather(hidden_share, "kv", axis=1, tiled=True),
        down_weight,
        preferred_element_type=jnp.float32,
    )
    mixer_out = lax.psum(mixer_part, "tp")
    return (mid_float + mixer_out).astype(jnp.bfloat16)


def solution(mesh):
    return jax.shard_map(
        local,
        mesh=mesh,
        in_specs=(
            P("dp", "kv"),
            P("kv"),
            P("kv", "tp"),
            P("dp", "kv", "tp", None, None),
            P("dp", "kv", "tp", None),
            P("tp"),
            P(),
            P("tp", "kv"),
            P("kv"),
            P("kv", "tp"),
            P("tp", "kv"),
        ),
        out_specs=P("dp", "kv"),
        check_vma=False,
    )
```

profile of v0, /device:TPU:0, one launch (start us, length us, event | category | flops | bytes accessed | tf_op | source)
XLA Modules:
  0.0 270.8 jit_solution(3176983266643035362)
XLA Ops:
  7.8 1.6 fusion.22
  9.4 34.9 %psum.20 = f32[8]{0:T(128)S(1)} all-reduce(f32[8]{0:T(128)S(1)} %fusion.19), channel_id=1, replica_groups=mesh['dp'=2,'kv'=16,'tp'=1] {'kv'}, use_global_device_ids=true, to_apply=%region_1.0 | all-reduce | flops 8 | bytes 64 | tf_op jit(solution)/shard_map/psum | solution.py:68
  44.4 55.3 %all-reduce.2.cloned.1.call-done = f32[8,2048]{1,0:T(8,128)} async-done(((f32[8,2048]{1,0:T(8,128)}), f32[8,2048]{1,0:T(8,128)}) %all-reduce.2.cloned.1.call-update) | async-done | bytes 65552 | tf_op jit(solution)/shard_map/psum | solution.py:69
  99.7 1.1 broadcast_multiply_fusion
  101.0 4.5 %fusion.5 = f32[8,8,2,1,128]{4,3,2,1,0:T(1,128)S(1)} fusion(bf16[8,128,8,2,128]{4,3,2,1,0:T(2,128)(2,1)} %param.16, bf16[8,8,2,128,1]{3,0,2,1,4:T(8,128)(2,1)S(1)} %maximum_bitcast_fusion), kind=kOutput, calls=%fused_computation.13 | convolution fusion | flops 4194304 | bytes 4292608 | tf_op jit(solution)/shard_map/bhcd,bkhcd->bhck/dot_general | solution.py:73
  107.4 22.6 %all-gather = f32[128,8,2]{1,2,0:T(2,128)S(1)} all-gather(f32[8,8,2]{1,2,0:T(2,128)S(1)} %copy.45), channel_id=2, replica_groups=mesh['dp'=2,'kv'=16,'tp'=1] {'kv'}, dimensions={0}, use_global_device_ids=true | all-gather | bytes 8704 | tf_op jit(solution)/shard_map/all_gather | solution.py:12
  130.4 18.1 %all-gather.1 = f32[128,8,2]{1,2,0:T(2,128)S(1)} all-gather(f32[8,8,2]{1,2,0:T(2,128)S(1)} %copy.46), channel_id=3, replica_groups=mesh['dp'=2,'kv'=16,'tp'=1] {'kv'}, dimensions={0}, use_global_device_ids=true | all-gather | bytes 8704 | tf_op jit(solution)/shard_map/all_gather | solution.py:12
  148.5 1.9 all-gather.5.cloned.1.call-done
  151.4 24.7 %while.19 = (s32[]{:T(128)}, f32[8,8,2]{1,0,2:T(8,128)S(1)}, f32[8,8,2]{1,0,2:T(8,128)S(1)}, f32[8,8,2,256]{3,2,1,0:T(2,128)S(1)}, f32[16,8,8,2]{2,3,1,0:T(2,128...) while((s32[]{:T(128)}, f32[8,8,2]{1,0,2:T(8,128)S(1)}, ...), condition=%wide.region_6.0_spmd, body=%wide.region_5.0_spmd.sunk | while | flops 99077 | bytes 664727 | solution.py:18
  151.5 0.9 constant_dynamic-slice_fusion.6
  153.1 0.9 constant_dynamic-slice_fusion.6
  154.8 0.9 constant_dynamic-slice_fusion.6
  156.4 0.9 constant_dynamic-slice_fusion.6
  158.1 0.9 constant_dynamic-slice_fusion.6
  159.7 0.9 constant_dynamic-slice_fusion.6
  161.4 0.9 constant_dynamic-slice_fusion.6
  163.0 0.9 constant_dynamic-slice_fusion.6
  164.6 0.9 constant_dynamic-slice_fusion.6
  166.3 0.9 constant_dynamic-slice_fusion.6
  177.4 5.4 %fusion.21 = f32[8,16384]{1,0:T(8,128)} fusion(bf16[256,16384]{1,0:T(8,128)(2,1)} %param.22, f32[8,256]{1,0:T(8,128)S(1)} %get-tuple-element.231, f32[256]{0:T(256)S(1)} %copy-done.4), kind=kOutput, calls=%fused_computation.46 | convolution fusion | flops 67112960 | bytes 8922112 | tf_op jit(solution)/shard_map/dot_general | solution.py:97
  182.8 31.6 %psum.24 = f32[8]{0:T(128)S(1)} all-reduce(f32[8]{0:T(128)S(1)} %get-tuple-element.230), channel_id=1, replica_groups=mesh['dp'=2,'kv'=16,'tp'=1] {'kv'}, use_global_device_ids=true, to_apply=%region_9.0 | all-reduce | flops 8 | bytes 64 | tf_op jit(solution)/shard_map/psum | solution.py:94
  214.4 23.7 %reduce-scatter.2.cloned.1.call-done = f32[8,1024]{1,0:T(8,128)} async-done(((f32[8,16384]{1,0:T(8,128)}), f32[8,1024]{1,0:T(8,128)}) %reduce-scatter.2.cloned.1.call-update) | async-done | bytes 32784 | tf_op jit(solution)/shard_map/reduce_scatter | solution.py:98
  239.0 20.1 %all_gather.27 = bf16[8,16384]{1,0:T(8,128)(2,1)S(1)} all-gather(bf16[8,1024]{1,0:T(8,128)(2,1)S(1)} %multiply_convert_fusion.2), channel_id=1, replica_groups=mesh['dp'=2,'kv'=16,'tp'=1] {'kv'}, dimensions={1}, use_global_device_ids=true | all-gather | bytes 278528 | tf_op jit(solution)/shard_map/all_gather | solution.py:101
  259.1 5.2 %fusion.11 = bf16[8,256]{1,0:T(8,128)(2,1)} fusion(f32[8,256]{1,0:T(8,128)S(1)} %get-tuple-element.231, bf16[8,16384]{1,0:T(8,128)(2,1)S(1)} %all_gather.27, bf16[16384,256]{1,0:T(8,128)(2,1)} %param.23), kind=kOutput, calls=%fused_computation.21 | convolution fusion | flops 67112960 | bytes 8663040 | tf_op jit(solution)/shard_map/dot_general | solution.py:100
  (134 shorter events, 21.9 us)
Async XLA Ops:
  6.5 1.2 copy-start
  6.5 93.2 %all-reduce.2.cloned.1.call-start = ((), (), s32[]{:S(2)}) async-start(), calls=%async_computation.1 | async-start | bytes 131072 | tf_op jit(solution)/shard_map/psum | solution.py:69
  9.4 141.1 %all-gather.5.cloned.1.call-start = ((), (), s32[]{:S(2)}) async-start(), calls=%async_computation.3 | async-start | bytes 2228224 | tf_op jit(solution)/shard_map/all_gather | solution.py:12
  99.7 5.9 %copy-start.1 = (bf16[8,128,8,256]{3,2,1,0:T(8,128)(2,1)S(1)}, bf16[8,128,8,256]{3,2,1,0:T(8,128)(2,1)}, u32[]{:S(2)}) copy-start(bf16[8,128,8,256]{3,2,1,0:T(8,128)(2,1)} %param.17) | copy-start | bytes 12582916
  100.9 6.2 %copy-start.6 = (f32[256]{0:T(256)S(1)}, f32[256]{0:T(256)}, u32[]{:S(2)}) copy-start(f32[256]{0:T(256)} %param.19) | copy-start | bytes 3076
  101.0 6.3 %copy-start.5 = (f32[8]{0:T(128)S(1)}, f32[8]{0:T(128)}, u32[]{:S(2)}) copy-start(f32[8]{0:T(128)} %param.18) | copy-start | bytes 100
  106.5 70.6 %copy-start.2 = (bf16[2048,256]{1,0:T(8,128)(2,1)S(1)}, bf16[2048,256]{1,0:T(8,128)(2,1)}, u32[]{:S(2)}) copy-start(bf16[2048,256]{1,0:T(8,128)(2,1)} %param.20) | copy-start | bytes 3145732
  106.5 70.6 %copy-start.3 = (bf16[8,256]{1,0:T(8,128)(2,1)S(1)}, bf16[8,256]{1,0:T(8,128)(2,1)}, u32[]{:S(2)}) copy-start(bf16[8,256]{1,0:T(8,128)(2,1)} %param.13) | copy-start | bytes 12292
  107.1 131.0 %reduce-scatter.2.cloned.1.call-start = ((), (), s32[]{:S(2)}) async-start(), calls=%async_computation.2 | async-start | bytes 557056 | tf_op jit(solution)/shard_map/reduce_scatter | solution.py:98
  107.4 70.0 %copy-start.4 = (f32[256]{0:T(256)S(1)}, f32[256]{0:T(256)}, u32[]{:S(2)}) copy-start(f32[256]{0:T(256)} %param.21) | copy-start | bytes 3076
Sparse Core Ops, SparseCore 0:
  10.8 88.8 all-reduce.1
  107.3 43.1 all-gather.4
  182.9 55.1 reduce-scatter.1
where the time goes:
time: 271 us
  blocking collectives  127 us (47%)
  waiting for transfers between devices  81 us (30%)
  local copies, waits for them, and re-layouts  20.5 us (8%)
  matrix products  17.8 us (7%)
  between operations  13.3 us (5%)
  other arithmetic  10.3 us (4%)
    psum x1, waiting for transfers between devices, local(): query_raw = lax.psum(query_part, 'kv')  55.3 us
    all_gather x2, blocking collectives, merged(): everything = jax.tree.map(lambda part: lax.all_gather(part, axis), value)  40.7 us
    psum x1, blocking collectives, local(): squares = lax.psum(own_squares, 'kv')  34.9 us
    psum x1, blocking collectives, local(): mix_squares = lax.psum(jnp.sum(mid_float * mid_float, axis=1), 'kv')  31.6 us
    reduce_scatter x1, waiting for transfers between devices, local(): share = lax.psum_scatter(up_part, 'kv', scatter_dimension=1, tiled=True)  23.7 us
    all_gather x1, blocking collectives, local(): lax.all_gather(hidden_share, 'kv', axis=1, tiled=True)  20.1 us
    dynamic_slice x30, local copies, waits for them, and re-layouts, lap(): return combine(so_far, jax.tree.map(lambda part: part[k], everything))  13.9 us
    add x15, other arithmetic, combine_partial(): numer_a * factor_a[..., None] + numer_b * factor_b[..., None]  6.36 us
  transfers between devices with their start and end apart: 3, of which 3 were waited for; matrix products, arithmetic and copies ran while one was open for 0% of the time, Pallas kernels for 0%

commit v1 on v0

--- a/solution.py
+++ b/solution.py
@@ -57,6 +57,11 @@
     up_weight,
     down_weight,
 ):
+
+    def supply_the_works(local_array, axis_key):
+        block_last = lax.all_gather(local_array, axis_key)
+        return jnp.sum(block_last, axis=0)
+
     row_count = tokens.shape[0]
     local_heads = key_cache.shape[2]
     head_width = key_cache.shape[4]
@@ -66,7 +71,7 @@
     scaled_in = (tok_float * attn_gain).astype(jnp.bfloat16)
     query_part = jnp.dot(scaled_in, query_weight, preferred_element_type=jnp.float32)
     squares = lax.psum(own_squares, "kv")
-    query_raw = lax.psum(query_part, "kv")
+    query_raw = supply_the_works(query_part, "kv")
     attn_inv = lax.rsqrt(squares / D + EPS)
     shaped = (attn_inv[:, None] * query_raw).reshape(row_count, local_heads, 2, head_width)
     query = rotate(shaped, length - 1).astype(jnp.bfloat16)

time: 271 us -> 220 us (0.81)
  waiting for transfers between devices: 81 us -> 31.1 us
  blocking collectives: 127 us -> 124 us
    psum x1 -> x0, waiting for transfers between devices: 55.3 us -> none  [local(): query_raw = lax.psum(query_part, 'kv')]
    all_gather x0 -> x1, waiting for transfers between devices: none -> 4.87 us  [supply_the_works(): block_last = lax.all_gather(local_array, axis_key)]
    all_gather x2, blocking collectives: 40.7 us -> 37.8 us  [merged(): everything = jax.tree.map(lambda part: lax.all_gather(part, axis), value)]
  transfers between devices with their start and end apart: 3 -> 3, of which waited for: 3 -> 3; matrix products, arithmetic and copies ran while one was open for 0% -> 1% of each run, Pallas kernels for 0% -> 0%
where the time goes in v1:
time: 220 us; the launch traced here: 219 us
  blocking collectives  124 us (56%)
  waiting for transfers between devices  31.1 us (14%)
  local copies, waits for them, and re-layouts  21.5 us (10%)
  matrix products  17.9 us (8%)
  between operations  13.3 us (6%)
  other arithmetic  10.5 us (5%)
    all_gather x2, blocking collectives, merged(): everything = jax.tree.map(lambda part: lax.all_gather(part, axis), value)  37.8 us
    psum x1, blocking collectives, local(): squares = lax.psum(own_squares, 'kv')  35 us
    psum x1, blocking collectives, local(): mix_squares = lax.psum(jnp.sum(mid_float * mid_float, axis=1), 'kv')  31.6 us
    reduce_scatter x1, waiting for transfers between devices, local(): share = lax.psum_scatter(up_part, 'kv', scatter_dimension=1, tiled=True)  23.7 us
    all_gather x1, blocking collectives, local(): lax.all_gather(hidden_share, 'kv', axis=1, tiled=True)  20.1 us
    dynamic_slice x30, local copies, waits for them, and re-layouts, lap(): return combine(so_far, jax.tree.map(lambda part: part[k], everything))  14 us
    add x15, other arithmetic, combine_partial(): numer_a * factor_a[..., None] + numer_b * factor_b[..., None]  6.36 us
    dot_general x1, matrix products, local(): up_part = jnp.dot(mixer_in, up_weight, preferred_element_type=jnp.float32)  5.37 us
  transfers between devices with their start and end apart: 3, of which 3 were waited for; matrix products, arithmetic and copies ran while one was open for 1% of the time, Pallas kernels for 0%

profile of v1, /device:TPU:0, one launch (start us, length us, event | category | flops | bytes accessed | tf_op | source)
XLA Modules:
  0.0 219.4 jit_solution(6100705474678047307)
XLA Ops:
  6.5 1.2 copy-done
  7.8 1.6 fusion.22
  10.2 35.0 %psum.14 = f32[8]{0:T(128)S(1)} all-reduce(f32[8]{0:T(128)S(1)} %fusion.19), channel_id=1, replica_groups=mesh['dp'=2,'kv'=16,'tp'=1] {'kv'}, use_global_device_ids=true, to_apply=%region_1.0 | all-reduce | flops 8 | bytes 64 | tf_op jit(solution)/shard_map/psum | solution.py:73
  45.3 4.9 %all-gather.7.cloned.1.call-done = f32[128,2048]{1,0:T(8,128)} async-done(((f32[8,2048]{1,0:T(8,128)}), f32[128,2048]{1,0:T(8,128)}) %all-gather.7.cloned.1.call-update) | async-done | bytes 1048592 | tf_op jit(solution)/shard_map/all_gather | solution.py:62
  50.1 1.3 bitcast_reduce_fusion
  51.8 4.6 %fusion.5 = f32[8,8,2,1,128]{4,3,2,1,0:T(1,128)S(1)} fusion(bf16[8,128,8,2,128]{4,3,2,1,0:T(2,128)(2,1)} %param.16, bf16[8,8,2,128,1]{3,1,2,0,4:T(8,128)(2,1)S(1)} %maximum_bitcast_fusion), kind=kOutput, calls=%fused_computation.13 | convolution fusion | flops 4194304 | bytes 4292608 | tf_op jit(solution)/shard_map/bhcd,bkhcd->bhck/dot_general | solution.py:78
  58.4 19.8 %all-gather.1 = f32[128,8,2]{1,2,0:T(2,128)S(1)} all-gather(f32[8,8,2]{1,2,0:T(2,128)S(1)} %copy.80), channel_id=3, replica_groups=mesh['dp'=2,'kv'=16,'tp'=1] {'kv'}, dimensions={0}, use_global_device_ids=true | all-gather | bytes 8704 | tf_op jit(solution)/shard_map/all_gather | solution.py:12
  78.6 17.9 %all-gather.2 = f32[128,8,2]{1,2,0:T(2,128)S(1)} all-gather(f32[8,8,2]{1,2,0:T(2,128)S(1)} %copy.81), channel_id=4, replica_groups=mesh['dp'=2,'kv'=16,'tp'=1] {'kv'}, dimensions={0}, use_global_device_ids=true | all-gather | bytes 8704 | tf_op jit(solution)/shard_map/all_gather | solution.py:12
  96.5 2.5 %all-gather.9.cloned.1.call-done = f32[128,8,2,256]{3,1,2,0:T(8,128)} async-done(((f32[8,8,2,256]{3,1,2,0:T(8,128)}), f32[128,8,2,256]{3,1,2,0:T(8,128)}) %all-gather.9.cloned.1.call-update) | async-done | bytes 2097168 | tf_op jit(solution)/shard_map/all_gather | solution.py:12
  100.1 24.7 %while.19 = (s32[]{:T(128)}, f32[8,8,2]{1,0,2:T(8,128)S(1)}, f32[8,8,2]{1,0,2:T(8,128)S(1)}, f32[8,8,2,256]{3,2,1,0:T(2,128)S(1)}, f32[16,8,8,2]{2,3,1,0:T(2,128...) while((s32[]{:T(128)}, f32[8,8,2]{1,0,2:T(8,128)S(1)}, ...), condition=%wide.region_6.0_spmd, body=%wide.region_5.0_spmd.sunk | while | flops 99077 | bytes 664727 | solution.py:18
  100.1 0.9 constant_dynamic-slice_fusion.6
  101.8 0.9 constant_dynamic-slice_fusion.6
  103.4 0.9 constant_dynamic-slice_fusion.6
  105.1 0.9 constant_dynamic-slice_fusion.6
  106.7 0.9 constant_dynamic-slice_fusion.6
  108.4 0.9 constant_dynamic-slice_fusion.6
  110.0 0.9 constant_dynamic-slice_fusion.6
  111.7 0.9 constant_dynamic-slice_fusion.6
  113.3 0.9 constant_dynamic-slice_fusion.6
  126.1 5.4 %fusion.21 = f32[8,16384]{1,0:T(8,128)} fusion(bf16[256,16384]{1,0:T(8,128)(2,1)} %param.22, f32[8,256]{1,0:T(8,128)S(1)} %get-tuple-element.245, f32[256]{0:T(256)S(1)} %copy-done.4), kind=kOutput, calls=%fused_computation.47 | convolution fusion | flops 67112960 | bytes 8922112 | tf_op jit(solution)/shard_map/dot_general | solution.py:102
  131.5 31.6 %psum.15 = f32[8]{0:T(128)S(1)} all-reduce(f32[8]{0:T(128)S(1)} %get-tuple-element.244), channel_id=1, replica_groups=mesh['dp'=2,'kv'=16,'tp'=1] {'kv'}, use_global_device_ids=true, to_apply=%region_9.0 | all-reduce | flops 8 | bytes 64 | tf_op jit(solution)/shard_map/psum | solution.py:99
  163.1 23.7 %reduce-scatter.2.cloned.1.call-done = f32[8,1024]{1,0:T(8,128)} async-done(((f32[8,16384]{1,0:T(8,128)}), f32[8,1024]{1,0:T(8,128)}) %reduce-scatter.2.cloned.1.call-update) | async-done | bytes 32784 | tf_op jit(solution)/shard_map/reduce_scatter | solution.py:103
  187.6 20.1 %all_gather.35 = bf16[8,16384]{1,0:T(8,128)(2,1)S(1)} all-gather(bf16[8,1024]{1,0:T(8,128)(2,1)S(1)} %multiply_convert_fusion.2), channel_id=1, replica_groups=mesh['dp'=2,'kv'=16,'tp'=1] {'kv'}, dimensions={1}, use_global_device_ids=true | all-gather | bytes 278528 | tf_op jit(solution)/shard_map/all_gather | solution.py:106
  207.7 5.2 %fusion.11 = bf16[8,256]{1,0:T(8,128)(2,1)} fusion(f32[8,256]{1,0:T(8,128)S(1)} %get-tuple-element.245, bf16[8,16384]{1,0:T(8,128)(2,1)S(1)} %all_gather.35, bf16[16384,256]{1,0:T(8,128)(2,1)} %param.23), kind=kOutput, calls=%fused_computation.21 | convolution fusion | flops 67112960 | bytes 8663040 | tf_op jit(solution)/shard_map/dot_general | solution.py:105
  (136 shorter events, 22.5 us)
Async XLA Ops:
  6.5 1.2 copy-start
  6.5 43.6 %all-gather.7.cloned.1.call-start = ((), (), s32[]{:S(2)}) async-start(), calls=%async_computation.2 | async-start | bytes 1114112 | tf_op jit(solution)/shard_map/all_gather | solution.py:62
  9.3 89.7 %all-gather.9.cloned.1.call-start = ((), (), s32[]{:S(2)}) async-start(), calls=%async_computation.3 | async-start | bytes 2228224 | tf_op jit(solution)/shard_map/all_gather | solution.py:12
  51.5 5.1 %copy-start.1 = (bf16[8,128,8,256]{3,2,1,0:T(8,128)(2,1)S(1)}, bf16[8,128,8,256]{3,2,1,0:T(8,128)(2,1)}, u32[]{:S(2)}) copy-start(bf16[8,128,8,256]{3,2,1,0:T(8,128)(2,1)} %param.17) | copy-start | bytes 12582916
  51.8 6.3 %copy-start.6 = (f32[256]{0:T(256)S(1)}, f32[256]{0:T(256)}, u32[]{:S(2)}) copy-start(f32[256]{0:T(256)} %param.19) | copy-start | bytes 3076
  51.8 6.4 %copy-start.5 = (f32[8]{0:T(128)S(1)}, f32[8]{0:T(128)}, u32[]{:S(2)}) copy-start(f32[8]{0:T(128)} %param.18) | copy-start | bytes 100
  57.4 68.3 %copy-start.2 = (bf16[2048,256]{1,0:T(8,128)(2,1)S(1)}, bf16[2048,256]{1,0:T(8,128)(2,1)}, u32[]{:S(2)}) copy-start(bf16[2048,256]{1,0:T(8,128)(2,1)} %param.20) | copy-start | bytes 3145732
  57.4 68.3 %copy-start.3 = (bf16[8,256]{1,0:T(8,128)(2,1)S(1)}, bf16[8,256]{1,0:T(8,128)(2,1)}, u32[]{:S(2)}) copy-start(bf16[8,256]{1,0:T(8,128)(2,1)} %param.13) | copy-start | bytes 12292
  58.1 128.7 %reduce-scatter.2.cloned.1.call-start = ((), (), s32[]{:S(2)}) async-start(), calls=%async_computation.1 | async-start | bytes 557056 | tf_op jit(solution)/shard_map/reduce_scatter | solution.py:103
  58.4 67.7 %copy-start.4 = (f32[256]{0:T(256)S(1)}, f32[256]{0:T(256)}, u32[]{:S(2)}) copy-start(f32[256]{0:T(256)} %param.21) | copy-start | bytes 3076
Sparse Core Ops, SparseCore 0:
  9.5 40.5 all-gather.6
  58.2 40.8 all-gather.8
  131.6 55.0 reduce-scatter.1
